TPU v7x, 32 devices: a whole 2x2x4 slice. The times are simulated.
32 devices in a mesh: sp: 4 (over z), fs: 2 (over y), tp: 4 (over x, core).
Axes of the slice: x: 2, y: 2, z: 4, core: 2. Of those that a mesh axis runs over, the one named last changes fastest.
Arguments:
- tokens: bfloat16 [2, 3072, 2304], P('fs', 'sp'), may hold values from -6 to 6
- norm_gain: float32 [2304], replicated, may hold values from 0.1 to 1.9
- query_weight: bfloat16 [2304, 2048], P(('sp', 'fs'), 'tp'), may hold values from -6 to 6
- key_weight: bfloat16 [2304, 512], P(('sp', 'fs'), 'tp'), may hold values from -6 to 6
- value_weight: bfloat16 [2304, 512], P(('sp', 'fs'), 'tp'), may hold values from -0.125 to 0.125
- outer_weight: bfloat16 [2304, 2048], P(('sp', 'fs'), 'tp'), may hold values from -0.125 to 0.125
- inner_weight: bfloat16 [2304, 2048], P(('sp', 'fs'), 'tp'), may hold values from -0.125 to 0.125
- signal_weight: bfloat16 [2304, 2048], P(('sp', 'fs'), 'tp'), may hold values from -0.125 to 0.125
- conv_taps: float32 [3, 2048], P(None, 'tp'), may hold values from -3 to 3
- sink_logit: float32 [32], P('tp'), may hold values from -4 to 4
Outputs:
- attn_out: bfloat16 [2, 3072, 2048], P('fs', 'sp', 'tp')
- conv_out: bfloat16 [2, 3072, 2048], P('fs', 'sp', 'tp')
- log_total: float32 [2, 32, 3072], P('fs', 'tp', 'sp')
All inputs are finite; a program needn't handle non-finite values.
Results may differ from a plain program's by a relative error of at most 0.014.
The roundings to bfloat16 on the way count: a program that leaves them out, or rounds other values in their place, can miss the bound.
Values may be sent and summed in bfloat16 or wider, within the bound.
A program may use at most 64 MiB of HBM per device.

v0:
```python
import math

import jax
import jax.numpy as jnp
from jax import lax
from jax.sharding import PartitionSpec as P

HEAD = 64
WINDOW = 128


EPSILON = 1e-06


def extended(value, sides, width):
    for axis, dim in sides:
        size, length = (lax.axis_size(axis), value.shape[dim])
        up = [(i, (i + 1) % size) for i in range(size - 1)]
        down = [(j, i) for i, j in up]
        last = lax.slice_in_dim(value, length - width, length, axis=dim)
        initial = lax.slice_in_dim(value, 0, width, axis=dim)
        before = lax.ppermute(last, axis, up)
        after = lax.ppermute(initial, axis, down)
        value = jnp.concatenate([before, value, after], axis=dim)
    return value


def normalized(tokens, norm_gain):
    values = tokens.astype(jnp.float32)
    scaling = lax.rsqrt(jnp.mean(values * values, axis=-1, keepdims=True) + EPSILON)
    return (values * scaling * norm_gain).astype(jnp.bfloat16)


def folding(normed):

    def add_portions(running, portions, offset):
        return tuple(
            (jnp.dot(normed, portion, preferred_element_type=jnp.float32) for portion in portions)
        )

    return add_portions


def empty_sums(normed, weights):
    return tuple((jnp.zeros((normed.shape[0], weight.shape[1]), jnp.float32) for weight in weights))


def rounded(results):
    return tuple((result.astype(jnp.bfloat16) for result in results))


def gate_product(inner_gate, signal):
    return (inner_gate.astype(jnp.float32) * signal.astype(jnp.float32)).astype(jnp.bfloat16)


def send_edges(key_proj, value_proj, product):
    stacked = jnp.concatenate([key_proj, value_proj], axis=1)
    window_rows = extended(stacked, (("sp", 0),), WINDOW)
    conv_rows = extended(product, (("sp", 0),), 1)
    return (window_rows, conv_rows)


def banded_attention(queries, window_rows, sink_logit, slopes, first_pos, seq_length):
    tok_count = queries.shape[0]
    kv_cols = window_rows.shape[1] // 2
    kv_heads = kv_cols // HEAD
    group_size = queries.shape[1] // (HEAD * kv_heads)
    block_count = tok_count // WINDOW
    query_blocks = queries.reshape(block_count, WINDOW, kv_heads, group_size, HEAD)
    key_rows = window_rows[:, :kv_cols].reshape(block_count + 2, WINDOW, kv_heads, HEAD)
    value_rows = window_rows[:, kv_cols:].reshape(block_count + 2, WINDOW, kv_heads, HEAD)
    key_span = jnp.concatenate([key_rows[:-2], key_rows[1:-1], key_rows[2:]], axis=1)
    value_span = jnp.concatenate([value_rows[:-2], value_rows[1:-1], value_rows[2:]], axis=1)
    scores = jnp.einsum(
        "bqkgd,bskd->bkgqs", query_blocks, key_span, preferred_element_type=jnp.float32
    ) * (1.0 / math.sqrt(HEAD))
    distance = jnp.arange(WINDOW)[:, None] - jnp.arange(3 * WINDOW)[None, :] + WINDOW
    key_pos = (
        first_pos
        - WINDOW
        + WINDOW * jnp.arange(block_count)[:, None]
        + jnp.arange(3 * WINDOW)[None, :]
    )
    inside = (jnp.abs(distance)[None] <= WINDOW) & ((key_pos >= 0) & (key_pos < seq_length))[
        :, None, :
    ]
    scores = scores - slopes.reshape(kv_heads, group_size, 1, 1) * jnp.abs(distance).astype(
        jnp.float32
    )
    scores = jnp.where(inside[:, None, None], scores, -jnp.inf)
    sink_grid = sink_logit.reshape(kv_heads, group_size, 1, 1)
    row_peak = jnp.maximum(jnp.max(scores, axis=-1, keepdims=True), sink_grid)
    weights = jnp.exp(scores - row_peak)
    row_total = jnp.sum(weights, axis=-1, keepdims=True) + jnp.exp(sink_grid - row_peak)
    weighted = jnp.einsum(
        "bkgqs,bskd->bqkgd",
        weights.astype(jnp.bfloat16),
        value_span,
        preferred_element_type=jnp.float32,
    )
    attended = (
        (weighted / row_total.transpose(0, 3, 1, 2, 4))
        .astype(jnp.bfloat16)
        .reshape(tok_count, kv_heads * group_size * HEAD)
    )
    log_total = (
        (row_peak + jnp.log(row_total))[..., 0]
        .transpose(1, 2, 0, 3)
        .reshape(kv_heads * group_size, tok_count)
    )
    return (attended, log_total)


def per_device(
    tokens,
    norm_gain,
    query_weight,
    key_weight,
    value_weight,
    outer_weight,
    inner_weight,
    signal_weight,
    conv_taps,
    sink_logit,
):
    normed = normalized(tokens[0], norm_gain)
    add_portions = folding(normed)
    all_sums = add_portions(
        empty_sums(
            normed,
            (query_weight, key_weight, value_weight, outer_weight, inner_weight, signal_weight),
        ),
        (
            lax.all_gather(query_weight, ("sp", "fs"), axis=0, tiled=True),
            lax.all_gather(key_weight, ("sp", "fs"), axis=0, tiled=True),
            lax.all_gather(value_weight, ("sp", "fs"), axis=0, tiled=True),
            lax.all_gather(outer_weight, ("sp", "fs"), axis=0, tiled=True),
            lax.all_gather(inner_weight, ("sp", "fs"), axis=0, tiled=True),
            lax.all_gather(signal_weight, ("sp", "fs"), axis=0, tiled=True),
        ),
        jnp.int32(0),
    )
    queries, key_proj, value_proj, outer_gate, inner_gate, signal = rounded(all_sums)
    product = gate_product(inner_gate, signal)
    window_rows, conv_rows = send_edges(key_proj, value_proj, product)
    tok_count = normed.shape[0]
    head_local = queries.shape[1] // HEAD
    head_index = lax.axis_index("tp") * head_local + jnp.arange(1, head_local + 1)
    slopes = jnp.exp2(-8.0 * head_index.astype(jnp.float32) / (head_local * lax.axis_size("tp")))
    first_pos = lax.axis_index("sp") * tok_count
    attended, log_total = banded_attention(
        queries, window_rows, sink_logit, slopes, first_pos, tok_count * lax.axis_size("sp")
    )
    mixed_conv = conv_taps[0] * conv_rows[0:tok_count].astype(jnp.float32)
    mixed_conv = mixed_conv + conv_taps[1] * conv_rows[1 : tok_count + 1].astype(jnp.float32)
    mixed_conv = mixed_conv + conv_taps[2] * conv_rows[2 : tok_count + 2].astype(jnp.float32)
    conv_out = (outer_gate.astype(jnp.float32) * mixed_conv).astype(jnp.bfloat16)
    return (attended[None], conv_out[None], log_total[None])


def solution(mesh):
    in_specs = (
        P("fs", "sp", None),
        P(),
        P(("sp", "fs"), "tp"),
        P(("sp", "fs"), "tp"),
        P(("sp", "fs"), "tp"),
        P(("sp", "fs"), "tp"),
        P(("sp", "fs"), "tp"),
        P(("sp", "fs"), "tp"),
        P(None, "tp"),
        P("tp"),
    )
    out_specs = (P("fs", "sp", "tp"), P("fs", "sp", "tp"), P("fs", "tp", "sp"))
    return jax.shard_map(
        per_device, mesh=mesh, in_specs=in_specs, out_specs=out_specs, check_vma=False
    )
```

profile of v0, /device:TPU:0, one launch (start us, length us, event | category | flops | bytes accessed | tf_op | source)
XLA Modules:
  0.0 244.9 jit_solution(4852538381520881118)
XLA Ops:
  7.2 0.0 all-gather.11.cloned.1.call-start
  7.2 0.7 all-gather.11.cloned.1.call-update
  7.9 0.0 all-gather.9.cloned.1.call-start
  8.0 0.7 all-gather.9.cloned.1.call-update
  8.7 0.0 all-gather.5.cloned.1.call-start
  8.7 0.7 all-gather.5.cloned.1.call-update
  9.4 0.0 all-gather.7.cloned.1.call-start
  9.5 2.9 %fusion.3 = f32[768]{0:T(1024)S(1)} fusion(bf16[1,768,2304]{2,1,0:T(8,128)(2,1)} %param.10), kind=kLoop, calls=%fused_computation.7 | loop fusion | flops 5307648 | bytes 3542016 | tf_op jit(solution)/shard_map/reduce_sum | solution.py:30
  12.4 0.0 copy-done.8
  12.4 34.7 %all_gather.18 = bf16[2304,128]{1,0:T(8,128)(2,1)S(1)} all-gather(bf16[288,128]{1,0:T(8,128)(2,1)S(1)} %copy-done.8), channel_id=1, replica_groups=mesh['sp'=4,'fs'=2,'tp'=4] {'sp','fs'}, dimensions={0}, use_global_device_ids=true | all-gather | bytes 663552 | tf_op jit(solution)/shard_map/all_gather | solution.py:135
  47.1 0.0 copy-done.9
  47.1 32.9 %all_gather.19 = bf16[2304,128]{1,0:T(8,128)(2,1)S(1)} all-gather(bf16[288,128]{1,0:T(8,128)(2,1)S(1)} %copy-done.9), channel_id=1, replica_groups=mesh['sp'=4,'fs'=2,'tp'=4] {'sp','fs'}, dimensions={0}, use_global_device_ids=true | all-gather | bytes 663552 | tf_op jit(solution)/shard_map/all_gather | solution.py:136
  80.0 0.9 fusion.5
  80.9 1.3 convolution_convert_fusion.4
  82.2 1.3 convolution_convert_fusion.5
  83.6 0.0 copy-start.11
  83.6 0.7 pad_maximum_fusion.9
  84.3 1.9 collective-permute-start
  86.2 1.3 collective-permute-start.1
  87.5 0.0 all-gather.7.cloned.1.call-update
  87.6 0.7 fusion.25
  88.2 0.7 fusion.24
  89.0 0.1 fusion.35
  89.0 1.9 broadcast_and_fusion
  90.9 2.3 broadcast_multiply_fusion
  93.2 0.6 fusion.41
  93.7 1.9 slice.84
  95.6 1.9 slice.78
  97.5 0.7 max.33
  98.2 1.7 copy.39
  99.9 1.7 copy.36
  101.5 0.0 collective-permute-done
  101.6 0.0 collective-permute-done.1
  101.6 2.1 pad_maximum_fusion.7
  103.7 1.9 slice.77
  105.5 1.7 copy.35
  107.2 1.9 slice.83
  109.1 1.7 copy.38
  110.7 1.9 slice.86
  112.6 1.7 copy.40
  114.3 1.9 slice.81
  116.1 1.7 copy.37
  117.8 4.5 %convolution_convert_fusion = bf16[768,512]{1,0:T(8,128)(2,1)} fusion(bf16[768,2304]{1,0:T(8,128)(2,1)S(1)} %fusion.5, bf16[2304,512]{1,0:T(8,128)(2,1)} %all-gather.11.cloned.1.call-done), kind=kOutput, calls=%fused_computation.19 | convolution fusion | flops 1812332544 | bytes 6684672 | tf_op jit(solution)/shard_map/dot_general | solution.py:38
  122.3 5.4 %all-gather.9.cloned.1.call-done = bf16[2304,512]{1,0:T(8,128)(2,1)} async-done(((bf16[288,512]{1,0:T(8,128)(2,1)}), bf16[2304,512]{1,0:T(8,128)(2,1)}) %all-gather.9.cloned.1.call-update) | async-done | bytes 2359312 | tf_op jit(solution)/shard_map/all_gather | solution.py:138
  127.7 3.8 %multiply_convert_fusion.1 = bf16[768,512]{1,0:T(8,128)(2,1)S(1)} fusion(bf16[768,512]{1,0:T(8,128)(2,1)} %convolution_convert_fusion, bf16[768,2304]{1,0:T(8,128)(2,1)S(1)} %fusion.5, bf16[2304,512]{1,0:T(8,128)(2,1)} %all-gather.9.cloned.1.call-done), kind=kOutput, calls=%fused_computation.18 | convolution fusion | flops 1813905408 | bytes 7471104 | tf_op jit(solution)/shard_map/dot_general | solution.py:38
  131.5 0.7 fusion.40
  132.2 4.0 %collective-permute-start.2 = (bf16[1,512]{1,0:T(2,128)(2,1)}, bf16[1,512]{1,0:T(2,128)(2,1)}, u32[]{:S(2)}, u32[]{:S(2)}) collective-permute-start(bf16[1,512]{1,0:T(2,128)(2,1)} %get-tuple-element.9), channel_id=1, source_target_pairs={{0,8},{8,16},{16,24},{1,9},{9,17},{17,25},{2,10},{10,18},{18,26},{... | collective-permute-start | bytes 3080 | tf_op jit(solution)/shard_map/ppermute | solution.py:22
  136.2 0.0 copy-done.13
  136.2 1.5 collective-permute-start.3
  137.6 42.6 %all-gather.5.cloned.1.call-done = bf16[2304,512]{1,0:T(8,128)(2,1)} async-done(((bf16[288,512]{1,0:T(8,128)(2,1)}), bf16[2304,512]{1,0:T(8,128)(2,1)}) %all-gather.5.cloned.1.call-update) | async-done | bytes 2359312 | tf_op jit(solution)/shard_map/all_gather | solution.py:134
  180.3 4.5 %convolution_convert_fusion.3 = bf16[768,512]{1,0:T(8,128)(2,1)} fusion(bf16[768,2304]{1,0:T(8,128)(2,1)S(1)} %fusion.5, bf16[2304,512]{1,0:T(8,128)(2,1)} %all-gather.5.cloned.1.call-done), kind=kOutput, calls=%fused_computation.22 | convolution fusion | flops 1812332544 | bytes 6684672 | tf_op jit(solution)/shard_map/dot_general | solution.py:38
  184.8 3.6 %reshape.138 = bf16[6,128,2,4,64]{4,3,2,1,0:T(4,128)(2,1)} reshape(bf16[768,512]{1,0:T(8,128)(2,1)} %convolution_convert_fusion.3) | data formatting | bytes 1572864 | tf_op jit(solution)/shard_map/reshape | solution.py:69
  188.4 4.5 %fusion.6 = (f32[6,2,4,128]{3,2,1,0:T(4,128)S(1)}, f32[6,2,384,128,4]{3,2,4,1,0:T(8,128)S(1)}) fusion(f32[2,4,128,384]{2,3,1,0:T(8,128)} %broadcast_multiply_fusion, pred[6,128,384]{1,2,0:T(8,128)(4,1)} %broadcast_and_fusion, bf16[6,128,2,4,64]{4,3,2,1,0:T(4,128)(2,1)} %reshape.138, bf16[6,128,2,64]{1,3,2,0:T(8,128)(2,1)} %copy.40, ...), kind=kOutput, calls=%fused_computation.10 | convolution fusion | flops 313190400 | bytes 12705792 | tf_op jit(solution)/shard_map/bqkgd,bskd->bkgqs/dot_general | solution.py:74
  192.9 0.1 broadcast_maximum_fusion
  193.0 2.7 %fusion.1 = f32[6,2,4,128]{3,2,1,0:T(4,128)S(1)} fusion(f32[6,2,384,128,4]{3,2,4,1,0:T(8,128)S(1)} %get-tuple-element.23, f32[6,2,4,128]{3,2,1,0:T(4,128)S(1)} %broadcast_maximum_fusion, f32[2,4,128,384]{2,3,1,0:T(8,128)S(1)} %copy-done.1, pred[6,128,384]{1,2,0:T(8,128)(4,1)S(1)} %copy-done.4), kind=kLoop, calls=%fused_computation.5 | loop fusion | flops 11790336 | bytes 11354112 | tf_op jit(solution)/shard_map/reduce_sum | solution.py:94
  195.7 0.1 fusion.32
  195.8 3.5 %fusion.10 = bf16[6,128,2,4,64]{1,4,3,2,0:T(8,128)(2,1)} fusion(f32[6,2,384,128,4]{3,2,4,1,0:T(8,128)S(1)} %get-tuple-element.23, f32[6,2,4,128]{3,2,1,0:T(4,128)S(1)} %broadcast_maximum_fusion, f32[2,4,128,384]{2,3,1,0:T(8,128)S(1)} %copy-done.1, pred[6,128,384]{1,2,0:T(8,128)(4,1)S(1)} %copy-done.4, f32[6,128,2,4]{1,3,2,0:T(4,128)S(1)} %fusion.32, ...), kind=kOutput, calls=%fused_computation.14 | convolution fusion | flops 316342272 | bytes 12730368 | tf_op jit(solution)/shard_map/bkgqs,bskd->bqkgd/dot_general | solution.py:95
  199.3 0.7 fusion.27
  200.0 3.4 %copy.52 = bf16[6,128,2,4,64]{4,3,2,1,0:T(4,128)(2,1)} copy(bf16[6,128,2,4,64]{1,4,3,2,0:T(8,128)(2,1)} %fusion.10) | data formatting | bytes 1572864
  203.4 3.8 %reshape.139 = bf16[1,768,512]{2,1,0:T(8,128)(2,1)} reshape(bf16[6,128,2,4,64]{4,3,2,1,0:T(4,128)(2,1)} %copy.52) | data formatting | bytes 1572864
  207.2 25.5 %all-gather.7.cloned.1.call-done = bf16[2304,512]{1,0:T(8,128)(2,1)} async-done(((bf16[288,512]{1,0:T(8,128)(2,1)}), bf16[2304,512]{1,0:T(8,128)(2,1)}) %all-gather.7.cloned.1.call-update) | async-done | bytes 2359312 | tf_op jit(solution)/shard_map/all_gather | solution.py:137
  232.7 0.0 collective-permute-done.2
  232.7 0.0 collective-permute-done.3
  232.7 5.7 %fusion.15 = bf16[1,768,512]{2,1,0:T(8,128)(2,1)} fusion(bf16[768,512]{1,0:T(8,128)(2,1)} %copy-done.13, bf16[1,512]{1,0:T(2,128)(2,1)} %collective-permute-done.3, bf16[1,512]{1,0:T(2,128)(2,1)} %collective-permute-done.2, f32[512]{0:T(512)S(1)} %bitcast.94, f32[512]{0:T(512)S(1)} %bitcast.95, f32[512]{0:T(512)S(1)} %bitcast.93, ...), kind=kOutput, calls=%fused_computation.25 | convolution fusion | flops 1819017216 | bytes 7479296 | tf_op jit(solution)/shard_map/dot_general | solution.py:38
  (28 shorter events, 0.1 us)
Async XLA Ops:
  7.2 5.2 %copy-start.8 = (bf16[288,128]{1,0:T(8,128)(2,1)S(1)}, bf16[288,128]{1,0:T(8,128)(2,1)}, u32[]{:S(2)}) copy-start(bf16[288,128]{1,0:T(8,128)(2,1)} %param.13) | copy-start | bytes 221188
  7.2 110.6 %all-gather.11.cloned.1.call-start = ((), (), s32[]{:S(2)}) async-start(), calls=%async_computation.3 | async-start | bytes 2654208 | tf_op jit(solution)/shard_map/all_gather | solution.py:139
  7.9 39.2 %copy-start.9 = (bf16[288,128]{1,0:T(8,128)(2,1)S(1)}, bf16[288,128]{1,0:T(8,128)(2,1)}, u32[]{:S(2)}) copy-start(bf16[288,128]{1,0:T(8,128)(2,1)} %param.14) | copy-start | bytes 221188
  7.9 119.8 %all-gather.9.cloned.1.call-start = ((), (), s32[]{:S(2)}) async-start(), calls=%async_computation.2 | async-start | bytes 2654208 | tf_op jit(solution)/shard_map/all_gather | solution.py:138
  8.7 171.6 %all-gather.5.cloned.1.call-start = ((), (), s32[]{:S(2)}) async-start(), calls=%async_computation | async-start | bytes 2654208 | tf_op jit(solution)/shard_map/all_gather | solution.py:134
  9.4 70.6 %copy-start.10 = (f32[2304]{0:T(1024)S(1)}, f32[2304]{0:T(1024)}, u32[]{:S(2)}) copy-start(f32[2304]{0:T(1024)} %param.11) | copy-start | bytes 27652
  9.4 223.3 %all-gather.7.cloned.1.call-start = ((), (), s32[]{:S(2)}) async-start(), calls=%async_computation.1 | async-start | bytes 2654208 | tf_op jit(solution)/shard_map/all_gather | solution.py:137
  9.5 70.6 %copy-start = (bf16[1,768,2304]{2,1,0:T(8,128)(2,1)S(1)}, bf16[1,768,2304]{2,1,0:T(8,128)(2,1)}, u32[]{:S(2)}) copy-start(bf16[1,768,2304]{2,1,0:T(8,128)(2,1)} %param.10) | copy-start | bytes 10616836
  82.2 2.1 copy-start.2
  83.6 0.8 copy-start.3
  83.6 9.6 %copy-start.11 = (f32[3,512]{1,0:T(4,128)S(1)}, f32[3,512]{1,0:T(4,128)}, u32[]{:S(2)}) copy-start(f32[3,512]{1,0:T(4,128)} %param.18) | copy-start | bytes 18436
  84.3 17.2 %collective-permute-start = (bf16[128,256]{0,1:T(8,128)(2,1)}, bf16[128,256]{0,1:T(8,128)(2,1)}, u32[]{:S(2)}, u32[]{:S(2)}) collective-permute-start(bf16[128,256]{0,1:T(8,128)(2,1)} %get-tuple-element.17), channel_id=1, source_target_pairs={{0,8},{8,16},{16,24},{1,9},{9,17},{17,25},{2,10},{10,18},{18,26},{... | collective-permute-start | bytes 196616 | tf_op jit(solution)/shard_map/ppermute | solution.py:22
  86.2 15.3 %collective-permute-start.1 = (bf16[128,256]{0,1:T(8,128)(2,1)}, bf16[128,256]{0,1:T(8,128)(2,1)}, u32[]{:S(2)}, u32[]{:S(2)}) collective-permute-start(bf16[128,256]{0,1:T(8,128)(2,1)} %get-tuple-element.18), channel_id=1, source_target_pairs={{8,0},{16,8},{24,16},{9,1},{17,9},{25,17},{10,2},{18,10},{26,18},{... | collective-permute-start | bytes 196616 | tf_op jit(solution)/shard_map/ppermute | solution.py:23
  131.5 4.6 %copy-start.13 = (bf16[768,512]{1,0:T(8,128)(2,1)}, bf16[768,512]{1,0:T(8,128)(2,1)S(1)}, u32[]{:S(2)}) copy-start(bf16[768,512]{1,0:T(8,128)(2,1)S(1)} %multiply_convert_fusion.1) | copy-start | bytes 2359300
  132.2 100.5 %collective-permute-start.2 = (bf16[1,512]{1,0:T(2,128)(2,1)}, bf16[1,512]{1,0:T(2,128)(2,1)}, u32[]{:S(2)}, u32[]{:S(2)}) collective-permute-start(bf16[1,512]{1,0:T(2,128)(2,1)} %get-tuple-element.9), channel_id=1, source_target_pairs={{0,8},{8,16},{16,24},{1,9},{9,17},{17,25},{2,10},{10,18},{18,26},{... | collective-permute-start | bytes 3080 | tf_op jit(solution)/shard_map/ppermute | solution.py:22
  136.2 96.5 %collective-permute-start.3 = (bf16[1,512]{1,0:T(2,128)(2,1)S(1)}, bf16[1,512]{1,0:T(2,128)(2,1)}, u32[]{:S(2)}, u32[]{:S(2)}) collective-permute-start(bf16[1,512]{1,0:T(2,128)(2,1)S(1)} %get-tuple-element.10), channel_id=1, source_target_pairs={{8,0},{16,8},{24,16},{9,1},{17,9},{25,17},{10,2},{18,10},{26,18},{... | collective-permute-start | bytes 3080 | tf_op jit(solution)/shard_map/ppermute | solution.py:23
  188.4 4.6 %copy-start.1 = (f32[2,4,128,384]{2,3,1,0:T(8,128)S(1)}, f32[2,4,128,384]{2,3,1,0:T(8,128)}, u32[]{:S(2)}) copy-start(f32[2,4,128,384]{2,3,1,0:T(8,128)} %broadcast_multiply_fusion) | copy-start | bytes 4718596
  188.4 4.6 %copy-start.4 = (pred[6,128,384]{1,2,0:T(8,128)(4,1)S(1)}, pred[6,128,384]{1,2,0:T(8,128)(4,1)}, u32[]{:S(2)}) copy-start(pred[6,128,384]{1,2,0:T(8,128)(4,1)} %broadcast_and_fusion) | copy-start | bytes 884740
  193.0 2.8 %copy-start.5 = (bf16[6,128,2,64]{1,3,2,0:T(8,128)(2,1)S(1)}, bf16[6,128,2,64]{1,3,2,0:T(8,128)(2,1)}, u32[]{:S(2)}) copy-start(bf16[6,128,2,64]{1,3,2,0:T(8,128)(2,1)} %copy.36) | copy-start | bytes 589828
  193.0 2.8 %copy-start.6 = (bf16[6,128,2,64]{1,3,2,0:T(8,128)(2,1)S(1)}, bf16[6,128,2,64]{1,3,2,0:T(8,128)(2,1)}, u32[]{:S(2)}) copy-start(bf16[6,128,2,64]{1,3,2,0:T(8,128)(2,1)} %copy.35) | copy-start | bytes 589828
  193.0 2.8 %copy-start.7 = (bf16[6,128,2,64]{1,3,2,0:T(8,128)(2,1)S(1)}, bf16[6,128,2,64]{1,3,2,0:T(8,128)(2,1)}, u32[]{:S(2)}) copy-start(bf16[6,128,2,64]{1,3,2,0:T(8,128)(2,1)} %copy.37) | copy-start | bytes 589828
  200.0 32.7 %copy-start.12 = (f32[1,512]{1,0:T(1,128)S(1)}, f32[1,512]{1,0:T(1,128)}, u32[]{:S(2)}) copy-start(f32[1,512]{1,0:T(1,128)} %get-tuple-element.21) | copy-start | bytes 6148
Sparse Core Ops, SparseCore 0:
  10.2 63.2 all-gather.10
  75.7 51.9 all-gather.8
  129.9 50.3 all-gather.4
  182.3 50.3 all-gather.6
where the time goes:
time: 246 us; the launch traced here: 245 us
  waiting for transfers between devices  75.6 us (31%)
  blocking collectives  67.6 us (27%)
  local copies, waits for them, and re-layouts  34 us (14%)
  matrix products  29.2 us (12%)
  other arithmetic  15.8 us (6%)
  between operations  14 us (6%)
  starting transfers between devices  8.78 us (4%)
    all_gather x1, waiting for transfers between devices, per_device(): lax.all_gather(query_weight, ('sp', 'fs'), axis=0, tiled=True)  42.6 us
    all_gather x1, blocking collectives, per_device(): lax.all_gather(key_weight, ('sp', 'fs'), axis=0, tiled=True)  34.7 us
    all_gather x1, blocking collectives, per_device(): lax.all_gather(value_weight, ('sp', 'fs'), axis=0, tiled=True)  32.9 us
    all_gather x1, waiting for transfers between devices, per_device(): lax.all_gather(outer_weight, ('sp', 'fs'), axis=0, tiled=True)  25.5 us
    dot_general x6, matrix products, add_portions(): jnp.dot(normed, portion, preferred_element_type=jnp.float32)  21.2 us
    unnamed x30, local copies, waits for them, and re-layouts  7.24 us
    ppermute x2, starting transfers between devices, extended(): before = lax.ppermute(last, axis, up)  5.89 us
    all_gather x1, waiting for transfers between devices, per_device(): lax.all_gather(inner_weight, ('sp', 'fs'), axis=0, tiled=True)  5.36 us
  transfers between devices with their start and end apart: 8, of which 3 were waited for; matrix products, arithmetic and copies ran while one was open for 30% of the time, Pallas kernels for 0%

commit v1 on v0

--- a/solution.py
+++ b/solution.py
@@ -1,8 +1,12 @@
 import math
+
+import functools
 
 import jax
 import jax.numpy as jnp
 from jax import lax
+from jax.experimental import pallas as pl
+from jax.experimental.pallas import tpu as pltpu
 from jax.sharding import PartitionSpec as P
 
 HEAD = 64
@@ -158,6 +162,591 @@
     return (attended[None], conv_out[None], log_total[None])
 
 
+MESH = pl.DeviceIdType.MESH
+GROUPS = 3
+FAR = -1e30
+
+
+def mega_kernel(
+    ns,
+    tokens,
+    gain,
+    qw,
+    kvw,
+    ow,
+    iw,
+    sw,
+    taps,
+    slopes,
+    sinks,
+    attn_out,
+    conv_out,
+    log_out,
+    toks,
+    wts,
+    stage_w,
+    qs,
+    kvs,
+    bias,
+    prod,
+    outer,
+    attn_st,
+    log_st,
+    conv_st,
+    load_sem,
+    stage_sem,
+    misc_sem,
+    y_send,
+    w_recv,
+    up_send,
+    dn_send,
+    tok_send,
+    tok_recv,
+    kv_send,
+    kv_recv,
+    pr_send,
+    pr_recv,
+    ret_send,
+    ret_recv,
+):
+    s, f, t = lax.axis_index("sp"), lax.axis_index("fs"), lax.axis_index("tp")
+    other = 1 - f
+    core = lax.rem(t, 2)
+    mate = t + 1 - 2 * core
+    rows = tokens.shape[0]
+    half_rows = rows // 2
+    depth = qw.shape[0]
+    qcols = qs.shape[2]
+    heads = qcols // HEAD
+    chans = prod.shape[3]
+    blocks = rows // WINDOW
+    pad = (prod.shape[2] - rows) // 2
+    up, down, across, beside = (s + 1, f, t), (s - 1, f, t), (s, other, t), (s, f, mate)
+    has_up, has_down = s < ns - 1, s > 0
+
+    barrier = pltpu.get_barrier_semaphore()
+
+    @pl.when(has_up)
+    def _():
+        pl.semaphore_signal(barrier, inc=1, device_id=up, device_id_type=MESH)
+
+    @pl.when(has_down)
+    def _():
+        pl.semaphore_signal(barrier, inc=1, device_id=down, device_id_type=MESH)
+
+    pl.semaphore_signal(barrier, inc=1, device_id=across, device_id_type=MESH)
+    pl.semaphore_signal(barrier, inc=1, device_id=beside, device_id_type=MESH)
+
+    def block_rows(blk):
+        return pl.ds(pl.multiple_of(blk * depth, 16), depth)
+
+    def loads(g, half, dest, sems):
+        if g == 0:
+            qc = pl.ds(pl.multiple_of(half * qcols, 128), qcols)
+            pairs = [
+                (qw.at[:, qc], dest.at[:, pl.ds(0, qcols)]),
+                (kvw.at[half], dest.at[:, pl.ds(qcols, 2 * HEAD)]),
+            ]
+        else:
+            c = pl.ds(pl.multiple_of(half * (2 * chans) + (g - 1) * chans, 128), chans)
+            pairs = [
+                (ref.at[:, c], dest.at[:, pl.ds(i * chans, chans)])
+                for i, ref in enumerate((iw, sw, ow))
+            ]
+        return [
+            pltpu.make_async_copy(a, b, sems.at[g, i]) for i, (a, b) in enumerate(pairs)
+        ]
+
+    mine = s * 2 + f
+    theirs = s * 2 + other
+    own_loads = [loads(g, f, wts.at[g, block_rows(mine)], load_sem) for g in range(GROUPS)]
+    out_loads = [loads(g, other, stage_w.at[g], stage_sem) for g in range(GROUPS)]
+    for g in range(GROUPS):
+        for c in out_loads[g] + own_loads[g]:
+            c.start()
+    tok_load = pltpu.make_async_copy(tokens, toks.at[f], misc_sem.at[0])
+    tok_load.start()
+
+    pl.semaphore_wait(
+        barrier, 2 + jnp.where(has_up, 1, 0) + jnp.where(has_down, 1, 0)
+    )
+
+    y_copies = []
+    for g in range(GROUPS):
+        for c in out_loads[g]:
+            c.wait()
+        copy = pltpu.make_async_remote_copy(
+            src_ref=stage_w.at[g],
+            dst_ref=wts.at[g, block_rows(mine)],
+            send_sem=y_send.at[g],
+            recv_sem=w_recv.at[g, mine],
+            device_id=across,
+            device_id_type=MESH,
+        )
+        copy.start()
+        y_copies.append(copy)
+        for c in own_loads[g]:
+            c.wait()
+    share = pl.ds(pl.multiple_of(core * half_rows, 16), half_rows)
+    rest = pl.ds(pl.multiple_of((1 - core) * half_rows, 16), half_rows)
+    tok_copy = pltpu.make_async_remote_copy(
+        src_ref=tokens.at[share],
+        dst_ref=toks.at[f, share],
+        send_sem=tok_send.at[0],
+        recv_sem=tok_recv.at[0],
+        device_id=across,
+        device_id_type=MESH,
+    )
+    tok_copy.start()
+
+    def incoming(g, blk):
+        return pltpu.make_async_remote_copy(
+            src_ref=wts.at[g, block_rows(blk)],
+            dst_ref=wts.at[g, block_rows(blk)],
+            send_sem=up_send.at[g, blk],
+            recv_sem=w_recv.at[g, blk],
+            device_id=across,
+            device_id_type=MESH,
+        )
+
+    def forward(g, blk, upward):
+        return pltpu.make_async_remote_copy(
+            src_ref=wts.at[g, block_rows(blk)],
+            dst_ref=wts.at[g, block_rows(blk)],
+            send_sem=(up_send if upward else dn_send).at[g, blk],
+            recv_sem=w_recv.at[g, blk],
+            device_id=up if upward else down,
+            device_id_type=MESH,
+        )
+
+    def relay_step(g, d, par):
+        side = f if par == 0 else other
+        if d == 0:
+            blk = s * 2 + side
+            if par == 1:
+                incoming(g, blk).wait_recv()
+
+            @pl.when(has_up)
+            def _():
+                forward(g, blk, True).start()
+
+            @pl.when(has_down)
+            def _():
+                forward(g, blk, False).start()
+
+            return
+
+        @pl.when(s - d >= 0)
+        def _():
+            blk = (s - d) * 2 + side
+            incoming(g, blk).wait_recv()
+
+            @pl.when(has_up)
+            def _():
+                forward(g, blk, True).start()
+
+        @pl.when(s + d < ns)
+        def _():
+            blk = (s + d) * 2 + side
+            incoming(g, blk).wait_recv()
+
+            @pl.when(has_down)
+            def _():
+                forward(g, blk, False).start()
+
+    def settle():
+        for g in range(GROUPS):
+            y_copies[g].wait_send()
+            for d in range(ns):
+                for par in range(2):
+                    side = f if par == 0 else other
+
+                    @pl.when((s - d >= 0) & has_up)
+                    def _():
+                        forward(g, (s - d) * 2 + side, True).wait_send()
+
+                    @pl.when((s + d < ns) & has_down)
+                    def _():
+                        forward(g, (s + d) * 2 + side, False).wait_send()
+
+    def norm_rows(seq):
+        @pl.loop(0, blocks)
+        def _(b):
+            at = pl.ds(pl.multiple_of(b * WINDOW, WINDOW), WINDOW)
+            values = toks[seq, at, :].astype(jnp.float32)
+            scaling = lax.rsqrt(jnp.mean(values * values, axis=-1, keepdims=True) + EPSILON)
+            toks[seq, at, :] = (values * scaling * gain[...]).astype(jnp.bfloat16)
+
+    mm_rows = rows // 2
+
+    def make_bias():
+        key = lax.broadcasted_iota(jnp.int32, (3 * WINDOW, WINDOW), 0)
+        query = lax.broadcasted_iota(jnp.int32, (3 * WINDOW, WINDOW), 1)
+        away = jnp.abs(query - key + WINDOW)
+        for h in range(heads):
+            slope = slopes[f * heads + h]
+            bias[h] = jnp.where(away <= WINDOW, -slope * away.astype(jnp.float32), FAR)
+
+    def project_qkv(seq):
+        @pl.loop(0, 2)
+        def _(b):
+            at = pl.multiple_of(b * mm_rows, WINDOW)
+            out = jnp.dot(
+                toks[seq, pl.ds(at, mm_rows), :], wts[0], preferred_element_type=jnp.float32
+            )
+            qs[seq, pl.ds(at, mm_rows), :] = out[:, :qcols].astype(jnp.bfloat16)
+            kvs[seq, pl.ds(at + WINDOW, mm_rows), :] = out[:, qcols:].astype(jnp.bfloat16)
+
+    def edge_copies(buf, seq, width, sends, recvs, slot):
+        length = buf.shape[1] if len(buf.shape) == 3 else buf.shape[2]
+        ref = buf.at[seq] if len(buf.shape) == 3 else buf.at[slot // 2, seq]
+        climb = pltpu.make_async_remote_copy(
+            src_ref=ref.at[pl.ds(length - 2 * width, width)],
+            dst_ref=ref.at[pl.ds(0, width)],
+            send_sem=sends.at[slot, 0],
+            recv_sem=recvs.at[slot, 0],
+            device_id=up,
+            device_id_type=MESH,
+        )
+        fall = pltpu.make_async_remote_copy(
+            src_ref=ref.at[pl.ds(width, width)],
+            dst_ref=ref.at[pl.ds(length - width, width)],
+            send_sem=sends.at[slot, 1],
+            recv_sem=recvs.at[slot, 1],
+            device_id=down,
+            device_id_type=MESH,
+        )
+        return ref, length, climb, fall
+
+    def edges_start(buf, seq, width, sends, recvs, slot):
+        ref, length, climb, fall = edge_copies(buf, seq, width, sends, recvs, slot)
+        blank = jnp.zeros((width, ref.shape[1]), jnp.bfloat16)
+
+        @pl.when(has_up)
+        def _():
+            climb.start()
+
+        @pl.when(has_down)
+        def _():
+            fall.start()
+
+        @pl.when(jnp.logical_not(has_up))
+        def _():
+            ref[pl.ds(length - width, width), :] = blank
+
+        @pl.when(jnp.logical_not(has_down))
+        def _():
+            ref[pl.ds(0, width), :] = blank
+
+    def edges_wait(buf, seq, width, sends, recvs, slot):
+        _, _, climb, fall = edge_copies(buf, seq, width, sends, recvs, slot)
+
+        @pl.when(has_up)
+        def _():
+            climb.wait_send()
+            fall.wait_recv()
+
+        @pl.when(has_down)
+        def _():
+            fall.wait_send()
+            climb.wait_recv()
+
+    def attend(seq, first, count):
+        @pl.loop(first, first + count)
+        def _(b):
+            at = pl.multiple_of(b * WINDOW, WINDOW)
+            kv = kvs[seq, pl.ds(at, 3 * WINDOW), :]
+            keys = kv[:, :HEAD]
+            values_t = kv.astype(jnp.float32).T[HEAD:, :].astype(jnp.bfloat16)
+            queries = qs[seq, pl.ds(at, WINDOW), :]
+            low = jnp.where((b == 0) & (s == 0), FAR, 0.0)
+            high = jnp.where((b == blocks - 1) & (s == ns - 1), FAR, 0.0)
+            outs = []
+            for h in range(heads):
+                query = queries[:, h * HEAD : (h + 1) * HEAD]
+                scores = lax.dot_general(
+                    keys, query, (((1,), (1,)), ((), ())), preferred_element_type=jnp.float32
+                )
+                scores = scores * (1.0 / math.sqrt(HEAD)) + bias[h]
+                scores = jnp.concatenate(
+                    [
+                        scores[:WINDOW] + low,
+                        scores[WINDOW : 2 * WINDOW],
+                        scores[2 * WINDOW :] + high,
+                    ],
+                    axis=0,
+                )
+                sink = sinks[f * heads + h]
+                peak = jnp.maximum(jnp.max(scores, axis=0, keepdims=True), sink)
+                weights = jnp.exp(scores - peak)
+                total = jnp.sum(weights, axis=0, keepdims=True) + jnp.exp(sink - peak)
+                mixed = jnp.dot(
+                    values_t, weights.astype(jnp.bfloat16), preferred_element_type=jnp.float32
+                )
+                outs.append(mixed / total)
+                log_st[seq, pl.ds(h, 1), pl.ds(at, WINDOW)] = peak + jnp.log(total)
+            stacked = jnp.concatenate(outs, axis=0)
+            attn_st[seq, pl.ds(at, WINDOW), :] = stacked.T.astype(jnp.bfloat16)
+
+    half_cols = pl.ds(pl.multiple_of(f * qcols, 128), qcols)
+
+    def hand_back(src, dst, slot, seq_is_own):
+        if seq_is_own:
+            return pltpu.make_async_copy(src, dst, misc_sem.at[1 + slot])
+        return pltpu.make_async_remote_copy(
+            src_ref=src,
+            dst_ref=dst,
+            send_sem=ret_send.at[slot],
+            recv_sem=ret_recv.at[slot],
+            device_id=across,
+            device_id_type=MESH,
+        )
+
+    def attn_return(own):
+        seq = f if own else other
+        return [
+            hand_back(attn_st.at[seq], attn_out.at[:, half_cols], 0, own),
+            hand_back(log_st.at[seq], log_out.at[f], 1, own),
+        ]
+
+    def conv_return(g, own):
+        seq = f if own else other
+        cols = pl.ds(pl.multiple_of(f * (2 * chans) + (g - 1) * chans, 128), chans)
+        return [hand_back(conv_st.at[g - 1, seq], conv_out.at[:, cols], 1 + g, own)]
+
+    def project_conv(g, seq):
+        @pl.loop(0, 2)
+        def _(b):
+            at = pl.multiple_of(b * mm_rows, WINDOW)
+            out = jnp.dot(
+                toks[seq, pl.ds(at, mm_rows), :], wts[g], preferred_element_type=jnp.float32
+            )
+            inner = out[:, :chans].astype(jnp.bfloat16).astype(jnp.float32)
+            signal = out[:, chans : 2 * chans].astype(jnp.bfloat16).astype(jnp.float32)
+            prod[g - 1, seq, pl.ds(at + pad, mm_rows), :] = (inner * signal).astype(jnp.bfloat16)
+            outer[seq, pl.ds(at, mm_rows), :] = out[:, 2 * chans :].astype(jnp.bfloat16)
+
+    def mix(g, seq):
+        cols = pl.ds(pl.multiple_of(f * (2 * chans) + (g - 1) * chans, 128), chans)
+        tap = taps[:, cols]
+        size = rows + 2 * pad
+        full = prod[g - 1, seq].astype(jnp.float32)
+        before = pltpu.roll(full, 1, 0)[pad : pad + rows]
+        after = pltpu.roll(full, size - 1, 0)[pad : pad + rows]
+        mixed = tap[0:1] * before + tap[1:2] * full[pad : pad + rows] + tap[2:3] * after
+        conv_st[g - 1, seq] = (outer[seq].astype(jnp.float32) * mixed).astype(jnp.bfloat16)
+
+    def begin(copies):
+        for c in copies:
+            c.start()
+
+    def pass_tokens():
+        return pltpu.make_async_remote_copy(
+            src_ref=toks.at[other, share],
+            dst_ref=toks.at[other, share],
+            send_sem=tok_send.at[1],
+            recv_sem=tok_recv.at[1],
+            device_id=beside,
+            device_id_type=MESH,
+        )
+
+    def take_tokens():
+        tok_copy.wait_recv()
+        pass_tokens().start()
+
+    def ready_tokens():
+        pass_tokens().wait_recv()
+        pass_tokens().wait_send()
+        norm_rows(other)
+
+    def first_own():
+        tok_load.wait()
+        norm_rows(f)
+
+    def kv_start(seq, slot):
+        edges_start(kvs, seq, WINDOW, kv_send, kv_recv, slot)
+
+    def kv_wait(seq, slot):
+        edges_wait(kvs, seq, WINDOW, kv_send, kv_recv, slot)
+
+    def pr_start(g, seq, slot):
+        edges_start(prod, seq, pad, pr_send, pr_recv, (g - 1) * 2 + slot)
+
+    def pr_wait(g, seq, slot):
+        edges_wait(prod, seq, pad, pr_send, pr_recv, (g - 1) * 2 + slot)
+
+    def qkv_own():
+        project_qkv(f)
+        kv_start(f, 0)
+
+    def qkv_other():
+        project_qkv(other)
+        kv_start(other, 1)
+
+    def finish_conv(g, own):
+        seq, slot = (f, 0) if own else (other, 1)
+        pr_wait(g, seq, slot)
+        mix(g, seq)
+        begin(conv_return(g, own))
+
+    def both_parts(g, own):
+        seq, slot = (f, 0) if own else (other, 1)
+        project_conv(g, seq)
+        pr_start(g, seq, slot)
+
+    third = blocks // 3 if blocks % 3 == 0 else blocks
+    parts = blocks // third
+
+    def attend_part(seq, i):
+        if i < parts:
+            attend(seq, i * third, third)
+
+    plan = {
+        (0, 0): [make_bias],
+        (0, 2): [first_own],
+        (1, 0): [qkv_own],
+        (1, 2): [lambda: kv_wait(f, 0), lambda: attend_part(f, 0)],
+        (1, 3): [lambda: attend_part(f, 1)],
+        (1, 4): [lambda: attend_part(f, 2), lambda: begin(attn_return(True))],
+        (1, 7): [take_tokens],
+        (2, 0): [lambda: both_parts(1, True)],
+        (2, 1): [ready_tokens],
+        (2, 2): [qkv_other, lambda: finish_conv(1, True)],
+        (2, 3): [lambda: both_parts(1, False)],
+        (2, 4): [lambda: kv_wait(other, 1), lambda: attend_part(other, 0)],
+        (2, 5): [lambda: attend_part(other, 1)],
+        (2, 6): [lambda: attend_part(other, 2), lambda: begin(attn_return(False))],
+        (2, 7): [lambda: finish_conv(1, False)],
+    }
+    spare = dict(plan)
+    for g in range(GROUPS):
+        for d in range(ns):
+            for par in range(2):
+                relay_step(g, d, par)
+                for piece in spare.pop((g, d * 2 + par), []):
+                    piece()
+        for key in sorted(k for k in spare if k[0] == g):
+            for piece in spare.pop(key):
+                piece()
+
+    both_parts(2, False)
+    finish_conv(2, False)
+    both_parts(2, True)
+    finish_conv(2, True)
+
+    tok_copy.wait_send()
+    settle()
+    for own in (True, False):
+        for c in attn_return(own) + conv_return(1, own) + conv_return(2, own):
+            c.wait()
+
+
+def fused_device(
+    ns,
+    tokens,
+    norm_gain,
+    query_weight,
+    key_weight,
+    value_weight,
+    outer_weight,
+    inner_weight,
+    signal_weight,
+    conv_taps,
+    sink_logit,
+):
+    rows, width = tokens.shape[1:]
+    depth, local = query_weight.shape
+    qcols = local // 2
+    heads = qcols // HEAD
+    chans = outer_weight.shape[1] // 4
+    head_local = 2 * heads
+    head_index = lax.axis_index("tp") * head_local + jnp.arange(1, head_local + 1)
+    slopes = jnp.exp2(-8.0 * head_index.astype(jnp.float32) / (head_local * lax.axis_size("tp")))
+    kv_weight = jnp.stack(
+        [
+            jnp.concatenate([w[:, i * HEAD : (i + 1) * HEAD] for w in (key_weight, value_weight)], 1)
+            for i in range(2)
+        ]
+    )
+    group_cols = qcols + 2 * HEAD
+    pad = 16
+    bf, f32 = jnp.bfloat16, jnp.float32
+    dma = pltpu.SemaphoreType.DMA
+    hbm = pl.BlockSpec(memory_space=pl.ANY)
+    vmem = pl.BlockSpec(memory_space=pltpu.VMEM)
+    smem = pl.BlockSpec(memory_space=pltpu.SMEM)
+    attended, conv, logs = pl.pallas_call(
+        functools.partial(mega_kernel, ns),
+        out_shape=(
+            jax.ShapeDtypeStruct((rows, local), bf),
+            jax.ShapeDtypeStruct((rows, 4 * chans), bf),
+            jax.ShapeDtypeStruct((2, heads, rows), f32),
+        ),
+        in_specs=[hbm, vmem, hbm, hbm, hbm, hbm, hbm, vmem, smem, smem],
+        out_specs=(hbm, hbm, hbm),
+        scratch_shapes=[
+            pltpu.VMEM((2, rows, width), bf),
+            pltpu.VMEM((GROUPS, width, group_cols), bf),
+            pltpu.VMEM((GROUPS, depth, group_cols), bf),
+            pltpu.VMEM((2, rows, qcols), bf),
+            pltpu.VMEM((2, rows + 2 * WINDOW, 2 * HEAD), bf),
+            pltpu.VMEM((heads, 3 * WINDOW, WINDOW), f32),
+            pltpu.VMEM((2, 2, rows + 2 * pad, chans), bf),
+            pltpu.VMEM((2, rows, chans), bf),
+            pltpu.VMEM((2, rows, qcols), bf),
+            pltpu.VMEM((2, heads, rows), f32),
+            pltpu.VMEM((2, 2, rows, chans), bf),
+            dma((GROUPS, 3)),
+            dma((GROUPS, 3)),
+            dma((5,)),
+            dma((GROUPS,)),
+            dma((GROUPS, 2 * ns)),
+            dma((GROUPS, 2 * ns)),
+            dma((GROUPS, 2 * ns)),
+            dma((2,)),
+            dma((2,)),
+            dma((2, 2)),
+            dma((2, 2)),
+            dma((4, 2)),
+            dma((4, 2)),
+            dma((4,)),
+            dma((4,)),
+        ],
+        compiler_params=pltpu.CompilerParams(
+            collective_id=0, has_side_effects=True, vmem_limit_bytes=48 << 20
+        ),
+    )(
+        tokens[0],
+        norm_gain[None],
+        query_weight,
+        kv_weight,
+        outer_weight,
+        inner_weight,
+        signal_weight,
+        conv_taps,
+        slopes,
+        sink_logit,
+    )
+    return (attended[None], conv[None], logs.reshape(1, head_local, rows))
+
+
+def fits(mesh, args):
+    tokens, query_weight, key_weight, outer_weight = (args[i] for i in (0, 2, 3, 5))
+    sp, fs, tp = (mesh.shape[a] for a in ("sp", "fs", "tp"))
+    rows = tokens.shape[1] // sp
+    return (
+        fs == 2
+        and tokens.shape[0] == fs
+        and tp % 2 == 0
+        and rows % (2 * WINDOW) == 0
+        and key_weight.shape[1] == 2 * HEAD * tp
+        and query_weight.shape[1] % (256 * tp) == 0
+        and outer_weight.shape[1] == 512 * tp
+        and query_weight.shape[1] == 512 * tp
+        and query_weight.shape[0] % (16 * sp * fs) == 0
+    )
+
+
 def solution(mesh):
     in_specs = (
         P("fs", "sp", None),
@@ -172,6 +761,13 @@
         P("tp"),
     )
     out_specs = (P("fs", "sp", "tp"), P("fs", "sp", "tp"), P("fs", "tp", "sp"))
-    return jax.shard_map(
-        per_device, mesh=mesh, in_specs=in_specs, out_specs=out_specs, check_vma=False
-    )
+
+    def run(*args):
+        body = per_device
+        if fits(mesh, args):
+            body = functools.partial(fused_device, mesh.shape["sp"])
+        return jax.shard_map(
+            body, mesh=mesh, in_specs=in_specs, out_specs=out_specs, check_vma=False
+        )(*args)
+
+    return run

time: 246 us -> 120 us (0.49)
  Pallas kernels: 0 us -> 108 us
  waiting for transfers between devices: 75.6 us -> 0 us
  blocking collectives: 67.6 us -> 0 us
  matrix products: 29.2 us -> 0 us
  local copies, waits for them, and re-layouts: 34 us -> 10.4 us
  other arithmetic: 15.8 us -> 0.14 us
  between operations: 14 us -> 0.69 us
  starting transfers between devices: 8.78 us -> 0 us
    pallas_call x0 -> x1, Pallas kernels: none -> 108 us  [fused_device(): pl.pallas_call(functools.partial(mega_kernel, ns), out_shape=(jax.ShapeDt...]
    all_gather x4 -> x0, waiting for transfers between devices: 73.5 us -> none  [the longest x1 42.6 us: per_device(): lax.all_gather(query_weight, ('sp', 'fs'), axis=0, tiled=True)]
    all_gather x2 -> x0, blocking collectives: 67.6 us -> none  [the longest x1 34.7 us: per_device(): lax.all_gather(key_weight, ('sp', 'fs'), axis=0, tiled=True)]
    dot_general x8 -> x0, matrix products: 29.2 us -> none  [the longest x6 21.2 us: add_portions(): jnp.dot(normed, portion, preferred_element_type=jnp.float32)]
    slice x14 -> x2, local copies, waits for them, and re-layouts: 22.4 us -> 2.09 us  [fused_device(): w[:, i * HEAD:(i + 1) * HEAD]]
    ppermute x4 -> x0, starting transfers between devices: 8.63 us -> none  [the longest x2 5.89 us: extended(): before = lax.ppermute(last, axis, up)]
    reduce_sum x2 -> x0, other arithmetic: 5.58 us -> none  [the longest x1 2.91 us: normalized(): jnp.mean(values * values, axis=-1, keepdims=True) + EPSILON]
    reshape x1, local copies, waits for them, and re-layouts: 3.61 us -> 0.62 us  [fused_device(): return (attended[None], conv[None], logs.reshape(1, head_local, rows))]
  transfers between devices with their start and end apart: 8 -> 0, of which waited for: 3 -> 0; matrix products, arithmetic and copies ran while one was open for 30% -> 0% of each run, Pallas kernels for 0% -> 0%
where the time goes in v1:
time: 120 us; the launch traced here: 119 us
  Pallas kernels  108 us (90%)
  local copies, waits for them, and re-layouts  10.4 us (9%)
    pallas_call x1, Pallas kernels, fused_device(): pl.pallas_call(functools.partial(mega_kernel, ns), out_shape=(jax.ShapeDt...  108 us
    unnamed x14, local copies, waits for them, and re-layouts  6.95 us

profile of v1, /device:TPU:0, one launch (start us, length us, event | category | flops | bytes accessed | tf_op | source)
XLA Modules:
  0.0 119.4 jit_solution(16885583508773986976)
XLA Ops:
  0.6 0.7 broadcast_in_dim.9.gain
  1.4 1.0 fusion
  2.4 1.0 fusion.1
  3.5 0.1 maximum_bitcast_fusion
  3.6 0.0 copy-start
  3.6 1.0 copy-done
  4.6 0.0 copy-start.1
  4.6 1.0 copy-done.1
  5.5 0.0 copy-start.2
  5.5 1.0 copy-done.2
  6.5 0.0 copy-start.3
  6.5 1.0 copy-done.3
  7.5 0.0 copy-start.4
  7.5 0.7 copy-done.4
  8.2 0.0 copy-start.5
  8.2 0.7 copy-done.5
  8.8 108.2 %shard_map.121 = (bf16[768,512]{1,0:T(8,128)(2,1)S(1)}, bf16[768,512]{1,0:T(8,128)(2,1)S(1)}, f32[2,4,768]{2,1,0:T(4,128)S(1)}) custom-call(bf16[768,2304]{1,0:T(8,128)(2,1)} %bitcast.9, f32[1,2304]{1,0:T(1,128)S(1)} %broadcast_in_dim.9.gain, bf16[288,512]{1,0:T(8,128)(2,1)S(1)} %copy-done, bf16[2,288,128]{2,1,0:T(8,128)(2,1)S(1)} %pad_maximum_fusion.kvw, ...), custom_call_target="tpu_custom_call" | custom-call | tf_op jit(solution)/shard_map/pallas_call | solution.py:678
  117.0 0.6 reshape.9
  117.6 0.9 copy.15
  118.5 0.9 copy.16
  (2 shorter events, 0.0 us)
Async XLA Ops:
  3.6 1.0 copy-start
  4.6 1.0 copy-start.1
  5.5 1.0 copy-start.2
  6.5 1.0 copy-start.3
  7.5 0.7 copy-start.4
  8.2 0.7 copy-start.5

commit v2 on v1

--- a/solution.py
+++ b/solution.py
@@ -172,7 +172,8 @@
     tokens,
     gain,
     qw,
-    kvw,
+    kw,
+    vw,
     ow,
     iw,
     sw,
@@ -245,7 +246,6 @@
             qc = pl.ds(pl.multiple_of(half * qcols, 128), qcols)
             pairs = [
                 (qw.at[:, qc], dest.at[:, pl.ds(0, qcols)]),
-                (kvw.at[half], dest.at[:, pl.ds(qcols, 2 * HEAD)]),
             ]
         else:
             c = pl.ds(pl.multiple_of(half * (2 * chans) + (g - 1) * chans, 128), chans)
@@ -266,6 +266,15 @@
             c.start()
     tok_load = pltpu.make_async_copy(tokens, toks.at[f], misc_sem.at[0])
     tok_load.start()
+
+    lane = lax.broadcasted_iota(jnp.int32, (depth, 2 * HEAD), 1)
+    k_full, v_full = kw[...].astype(jnp.float32), vw[...].astype(jnp.float32)
+    low_pair = jnp.where(lane < HEAD, k_full, pltpu.roll(v_full, HEAD, 1))
+    high_pair = jnp.where(lane < HEAD, pltpu.roll(k_full, HEAD, 1), v_full)
+    first = f == 0
+    kv_cols = pl.ds(qcols, 2 * HEAD)
+    stage_w[0, :, kv_cols] = jnp.where(first, high_pair, low_pair).astype(jnp.bfloat16)
+    wts[0, block_rows(mine), kv_cols] = jnp.where(first, low_pair, high_pair).astype(jnp.bfloat16)
 
     pl.semaphore_wait(
         barrier, 2 + jnp.where(has_up, 1, 0) + jnp.where(has_down, 1, 0)
@@ -601,33 +610,59 @@
         if i < parts:
             attend(seq, i * third, third)
 
-    plan = {
-        (0, 0): [make_bias],
-        (0, 2): [first_own],
-        (1, 0): [qkv_own],
+    def attend_all(seq, own):
+        for i in range(parts):
+            attend_part(seq, i)
+        begin(attn_return(own))
+
+    start_plan = {(0, 0): [make_bias], (0, 2): [first_own], (1, 1): [qkv_own]}
+    end_plan = {
         (1, 2): [lambda: kv_wait(f, 0), lambda: attend_part(f, 0)],
         (1, 3): [lambda: attend_part(f, 1)],
         (1, 4): [lambda: attend_part(f, 2), lambda: begin(attn_return(True))],
-        (1, 7): [take_tokens],
+        (1, 6): [take_tokens],
         (2, 0): [lambda: both_parts(1, True)],
-        (2, 1): [ready_tokens],
-        (2, 2): [qkv_other, lambda: finish_conv(1, True)],
-        (2, 3): [lambda: both_parts(1, False)],
-        (2, 4): [lambda: kv_wait(other, 1), lambda: attend_part(other, 0)],
-        (2, 5): [lambda: attend_part(other, 1)],
-        (2, 6): [lambda: attend_part(other, 2), lambda: begin(attn_return(False))],
-        (2, 7): [lambda: finish_conv(1, False)],
+        (2, 1): [ready_tokens, qkv_other, lambda: both_parts(1, False)],
+        (2, 2): [lambda: kv_wait(other, 1), lambda: attend_part(other, 0)],
+        (2, 3): [lambda: attend_part(other, 1)],
+        (2, 4): [lambda: attend_part(other, 2), lambda: begin(attn_return(False))],
+        (2, 5): [lambda: finish_conv(1, False)],
+        (2, 6): [lambda: finish_conv(1, True)],
     }
-    spare = dict(plan)
+    inner_plan = {
+        (1, 5): [lambda: kv_wait(f, 0), lambda: attend_part(f, 0)],
+        (2, 1): [
+            lambda: attend_part(f, 1),
+            lambda: attend_part(f, 2),
+            lambda: begin(attn_return(True)),
+        ],
+        (2, 3): [lambda: both_parts(1, True), take_tokens],
+        (2, 5): [
+            ready_tokens,
+            qkv_other,
+            lambda: both_parts(1, False),
+            lambda: kv_wait(other, 1),
+            lambda: attend_all(other, False),
+            lambda: finish_conv(1, False),
+            lambda: finish_conv(1, True),
+        ],
+    }
+
+    def run_all(pieces):
+        for piece in pieces:
+            piece()
+
+    is_end = (s == 0) | (s == ns - 1)
     for g in range(GROUPS):
         for d in range(ns):
             for par in range(2):
                 relay_step(g, d, par)
-                for piece in spare.pop((g, d * 2 + par), []):
-                    piece()
-        for key in sorted(k for k in spare if k[0] == g):
-            for piece in spare.pop(key):
-                piece()
+                key = (g, d * 2 + par)
+                run_all(start_plan.get(key, []))
+                if key in end_plan:
+                    pl.when(is_end)(functools.partial(run_all, end_plan[key]))
+                if key in inner_plan:
+                    pl.when(jnp.logical_not(is_end))(functools.partial(run_all, inner_plan[key]))
 
     both_parts(2, False)
     finish_conv(2, False)
@@ -662,12 +697,6 @@
     head_local = 2 * heads
     head_index = lax.axis_index("tp") * head_local + jnp.arange(1, head_local + 1)
     slopes = jnp.exp2(-8.0 * head_index.astype(jnp.float32) / (head_local * lax.axis_size("tp")))
-    kv_weight = jnp.stack(
-        [
-            jnp.concatenate([w[:, i * HEAD : (i + 1) * HEAD] for w in (key_weight, value_weight)], 1)
-            for i in range(2)
-        ]
-    )
     group_cols = qcols + 2 * HEAD
     pad = 16
     bf, f32 = jnp.bfloat16, jnp.float32
@@ -682,7 +711,7 @@
             jax.ShapeDtypeStruct((rows, 4 * chans), bf),
             jax.ShapeDtypeStruct((2, heads, rows), f32),
         ),
-        in_specs=[hbm, vmem, hbm, hbm, hbm, hbm, hbm, vmem, smem, smem],
+        in_specs=[hbm, vmem, hbm, vmem, vmem, hbm, hbm, hbm, vmem, smem, smem],
         out_specs=(hbm, hbm, hbm),
         scratch_shapes=[
             pltpu.VMEM((2, rows, width), bf),
@@ -713,13 +742,14 @@
             dma((4,)),
         ],
         compiler_params=pltpu.CompilerParams(
-            collective_id=0, has_side_effects=True, vmem_limit_bytes=48 << 20
+            collective_id=0, has_side_effects=True, vmem_limit_bytes=63 << 20
         ),
     )(
         tokens[0],
         norm_gain[None],
         query_weight,
-        kv_weight,
+        key_weight,
+        value_weight,
         outer_weight,
         inner_weight,
         signal_weight,
@@ -736,6 +766,7 @@
     rows = tokens.shape[1] // sp
     return (
         fs == 2
+        and sp == 4
         and tokens.shape[0] == fs
         and tp % 2 == 0
         and rows % (2 * WINDOW) == 0

time: 120 us -> 126 us (1.050)
  Pallas kernels: 108 us -> 118 us
  local copies, waits for them, and re-layouts: 10.4 us -> 6.79 us
    pallas_call x1, Pallas kernels: 108 us -> 118 us  [fused_device(): pl.pallas_call(functools.partial(mega_kernel, ns), out_shape=(jax.ShapeDt...]
    unnamed x14 -> x2, local copies, waits for them, and re-layouts: 6.95 us -> 4.12 us
    slice x2 -> x0, local copies, waits for them, and re-layouts: 2.09 us -> none  [fused_device(): w[:, i * HEAD:(i + 1) * HEAD]]
where the time goes in v2:
time: 126 us
  Pallas kernels  118 us (94%)
  local copies, waits for them, and re-layouts  6.79 us (5%)
    pallas_call x1, Pallas kernels, fused_device(): pl.pallas_call(functools.partial(mega_kernel, ns), out_shape=(jax.ShapeDt...  118 us
    unnamed x2, local copies, waits for them, and re-layouts  4.12 us

profile of v2, /device:TPU:0, one launch (start us, length us, event | category | flops | bytes accessed | tf_op | source)
XLA Modules:
  0.0 125.6 jit_solution(2286597460656371466)
XLA Ops:
  0.6 0.5 multiply_exponential_fusion.slopes
  1.2 1.3 %broadcast_in_dim.9.gain = f32[1,2304]{1,0:T(1,128)} reshape(f32[2304]{0:T(1024)} %param.11) | data formatting | bytes 18432 | tf_op jit(solution)/shard_map/broadcast_in_dim | solution.py:749
  2.5 117.7 %shard_map.121 = (bf16[768,512]{1,0:T(8,128)(2,1)}, bf16[768,512]{1,0:T(8,128)(2,1)}, f32[2,4,768]{2,1,0:T(4,128)}) custom-call(bf16[768,2304]{1,0:T(8,128)(2,1)} %bitcast.3, f32[1,2304]{1,0:T(1,128)} %broadcast_in_dim.9.gain, bf16[288,512]{1,0:T(8,128)(2,1)} %qw.1, bf16[288,128]{1,0:T(8,128)(2,1)} %kw.1, bf16[288,128]{1,0:T(8,128)(2,1)} %vw.1, ...), custom_call_target="tpu_custom_call" | custom-call | tf_op jit(solution)/shard_map/pallas_call | solution.py:707
  120.1 1.4 %reshape.9 = f32[1,8,768]{2,1,0:T(8,128)} reshape(f32[2,4,768]{2,1,0:T(4,128)} %get-tuple-element.8) | data formatting | bytes 49152 | tf_op jit(solution)/shard_map/reshape | solution.py:760
  121.5 2.1 %copy.15 = bf16[1,768,512]{2,1,0:T(8,128)(2,1)} copy(bf16[1,768,512]{2,1,0:T(8,128)(2,1)} %bitcast.5) | data formatting | bytes 1572864
  123.6 2.1 %copy.16 = bf16[1,768,512]{2,1,0:T(8,128)(2,1)} copy(bf16[1,768,512]{2,1,0:T(8,128)(2,1)} %bitcast.4) | data formatting | bytes 1572864
